TPU v7x, 128 devices: a whole 4x4x4 slice. The times are simulated.
128 devices in a mesh: sp: 64 (over z, y, x), tp: 2 (over core).
Axes of the slice: x: 4, y: 4, z: 4, core: 2. Of those that a mesh axis runs over, the one named last changes fastest.
Arguments:
- residual: bfloat16 [16384, 2048], P(('sp', 'tp')), may hold values from -6 to 6
- queries: bfloat16 [16384, 1152], P('sp', 'tp'), may hold values from -800 to 800
- latent: bfloat16 [16384, 256], P('sp'), may hold values from -6 to 6
- rope_key: bfloat16 [16384, 32], P('sp'), may hold values from -6 to 6
- doc_ids: int32 [16384], P('sp'), may hold values from 0 to 5, never falling along the last dimension, each value on 1 to 8192 neighbouring positions
- latent_to_key: bfloat16 [256, 768], P(None, 'tp'), may hold values from -0.375 to 0.375
- latent_to_value: bfloat16 [256, 768], P(None, 'tp'), may hold values from -0.375 to 0.375
- out_proj: bfloat16 [768, 2048], replicated, may hold values from -0.21875 to 0.21875
- mix_gain: float32 [2048], replicated, may hold values from 0.1 to 1.9
- moe_gain: float32 [2048], replicated, may hold values from 0.1 to 1.9
- expert_ids: int32 [16384, 2], P(('sp', 'tp')), may hold values from 0 to 63, as said below
- route_weight: float32 [16384, 2], P(('sp', 'tp')), may hold values from 0.1 to 1
- gate_weight: bfloat16 [64, 2048, 1024], P('sp', None, 'tp'), may hold values from -0.125 to 0.125
- up_weight: bfloat16 [64, 2048, 1024], P('sp', None, 'tp'), may hold values from -0.125 to 0.125
- down_weight: bfloat16 [64, 1024, 2048], P('sp', 'tp'), may hold values from -0.1875 to 0.1875
Outputs:
- output: bfloat16 [16384, 2048], P(('sp', 'tp'))
Inputs may be any that keep to these rules, and one draw needn't show every extreme that they name: `expert_ids`: each row names 2 different experts of one group of 16 consecutive numbers; in each aligned block of 128 rows (the rows of one device) no expert is named more than 8 times, and some expert exactly 8 times.
All inputs are finite; a program needn't handle non-finite values.
Results may differ from a plain program's by a relative error of at most 0.013.
Values may be sent and summed in bfloat16 or wider, within the bound.
A program may use at most 64 MiB of HBM per device.

v0:
```python
import math
import jax
import jax.numpy as jnp
from jax import lax
from jax.sharding import PartitionSpec as P

D = 2048
UNROTATED_DIM = 64
ROPE = 32
VALUE_ENTRIES = 64
GROUPS = 4
rope_base = 10000.0
epsilon = 1e-06


def in_order(pieces, dim):
    pieces = jnp.moveaxis(pieces, 0, dim)
    lengths = pieces.shape
    return pieces.reshape(*lengths[:dim], lengths[dim] * lengths[dim + 1], *lengths[dim + 2 :])


def sent_to_all(x, axis):
    size = lax.axis_size(axis)
    return lax.all_to_all(jnp.broadcast_to(x[None], (size, *x.shape)), axis, 0, 0, tiled=True)


def collect(x, axis, dim):
    return in_order(sent_to_all(x, axis), dim)


def cut_along(x, dim, size):
    before, after = (x.shape[:dim], x.shape[dim + 1 :])
    return jnp.moveaxis(x.reshape(*before, size, -1, *after), dim, 0)


def sum_at_owner(x, axis, dim):
    pieces = cut_along(x, dim, lax.axis_size(axis))
    arrived = lax.all_to_all(pieces, axis, split_axis=0, concat_axis=0, tiled=True)
    return arrived.astype(jnp.float32).sum(axis=0)


def rotate(source, positions):
    half_width = source.shape[-1] // 2
    frequency = rope_base ** (-jnp.arange(half_width, dtype=jnp.float32) / half_width)
    angles = positions.astype(jnp.float32)[:, None] * frequency[None, :]
    if source.ndim == 3:
        angles = angles[:, None, :]
    cosine = jnp.cos(angles)
    sine_part = jnp.sin(angles)
    upper_half = source[..., :half_width].astype(jnp.float32)
    lower_half = source[..., half_width:].astype(jnp.float32)
    turned = jnp.concatenate(
        [
            upper_half * cosine - lower_half * sine_part,
            lower_half * cosine + upper_half * sine_part,
        ],
        axis=-1,
    )
    return turned.astype(jnp.bfloat16)


def rms_scale(source, gain):
    return source * lax.rsqrt(jnp.mean(source * source, axis=-1, keepdims=True) + epsilon) * gain


def attend_keys(
    running,
    query_nope,
    query_rot,
    query_pos,
    query_docs,
    key_nope,
    key_rot,
    value_rows,
    key_pos,
    key_docs,
):
    row_max, row_total, weighted = running
    score_scale = (UNROTATED_DIM + ROPE) ** (-0.5)
    scores = (
        jnp.einsum("qhd,khd->qhk", query_nope, key_nope, preferred_element_type=jnp.float32)
        + jnp.einsum("qhr,kr->qhk", query_rot, key_rot, preferred_element_type=jnp.float32)
    ) * score_scale
    allowed = (
        (key_pos[None, :] <= query_pos[:, None]) & (key_docs[None, :] == query_docs[:, None])
    )[:, None, :]
    new_max = jnp.maximum(row_max, jnp.max(jnp.where(allowed, scores, -1e30), axis=-1))
    weights = jnp.where(allowed, jnp.exp(scores - new_max[..., None]), 0.0)
    factor = jnp.exp(row_max - new_max)
    row_total = row_total * factor + jnp.sum(weights, axis=-1)
    weighted = weighted * factor[..., None] + jnp.einsum(
        "qhk,khd->qhd", weights.astype(jnp.bfloat16), value_rows, preferred_element_type=jnp.float32
    )
    return (new_max, row_total, weighted)


def local(
    residual,
    queries,
    latent,
    rope_key,
    doc_ids,
    latent_to_key,
    latent_to_value,
    out_proj,
    mix_gain,
    moe_gain,
    expert_ids,
    route_weight,
    gate_weight,
    up_weight,
    down_weight,
):
    local_rows = queries.shape[0]
    local_heads = queries.shape[1] // (UNROTATED_DIM + ROPE)
    query_pos = lax.axis_index("sp") * local_rows + jnp.arange(local_rows, dtype=jnp.int32)
    shaped = queries.reshape(local_rows, local_heads, UNROTATED_DIM + ROPE)
    query_nope = shaped[..., :UNROTATED_DIM]
    query_rot = rotate(shaped[..., UNROTATED_DIM:], query_pos)
    key_rot = rotate(rope_key, query_pos)
    initial = (
        jnp.full((local_rows, local_heads), -1e30, jnp.float32),
        jnp.zeros((local_rows, local_heads), jnp.float32),
        jnp.zeros((local_rows, local_heads, VALUE_ENTRIES), jnp.float32),
    )
    pieces = (
        lax.all_gather(latent, "sp", axis=0, tiled=True),
        lax.all_gather(key_rot, "sp", axis=0, tiled=True),
        lax.all_gather(doc_ids, "sp", axis=0, tiled=True),
    )
    row_count = pieces[0].shape[0]
    block_rows = math.gcd(row_count, 512)

    def one_block(number, current):
        first_row = number * block_rows
        sliced = [lax.dynamic_slice_in_dim(member, first_row, block_rows, 0) for member in pieces]
        key_pos = first_row + jnp.arange(block_rows, dtype=jnp.int32)
        active = (first_row <= query_pos[-1]) & (sliced[-1][-1] >= doc_ids[0])

        def compute(carried):
            key_nope = jnp.dot(sliced[0], latent_to_key, preferred_element_type=jnp.float32).astype(
                jnp.bfloat16
            )
            value_rows = jnp.dot(
                sliced[0], latent_to_value, preferred_element_type=jnp.float32
            ).astype(jnp.bfloat16)
            key_part = sliced[1]
            return attend_keys(
                carried,
                query_nope,
                query_rot,
                query_pos,
                doc_ids,
                key_nope.reshape(block_rows, local_heads, UNROTATED_DIM),
                key_part,
                value_rows.reshape(block_rows, local_heads, VALUE_ENTRIES),
                key_pos,
                sliced[-1],
            )

        return lax.cond(active, compute, lambda carried: carried, current)

    running = lax.fori_loop(0, row_count // block_rows, one_block, initial)
    attended = (running[2] / running[1][..., None]).astype(jnp.bfloat16)
    attended = attended.reshape(local_rows, local_heads * VALUE_ENTRIES)
    gathered = lax.all_to_all(attended, "tp", split_axis=0, concat_axis=1, tiled=True)
    mix = jnp.dot(gathered, out_proj, preferred_element_type=jnp.float32)
    branch = rms_scale(mix, mix_gain)
    middle = lax.optimization_barrier((residual.astype(jnp.float32) + branch).astype(jnp.bfloat16))
    normed = rms_scale(middle.astype(jnp.float32), moe_gain).astype(jnp.bfloat16)
    row_count = normed.shape[0]
    top_count = expert_ids.shape[1]
    expert_count = lax.axis_size("sp")
    capacity = row_count // (expert_count // GROUPS)
    flat_ids = expert_ids.reshape(-1)
    onehot = (flat_ids[:, None] == jnp.arange(expert_count, dtype=jnp.int32)[None, :]).astype(
        jnp.int32
    )
    earlier = jnp.cumsum(onehot, axis=0) - onehot
    slot_rank = jnp.sum(earlier * onehot, axis=1)
    slot_ids = (flat_ids * capacity + slot_rank).reshape(row_count, top_count)
    chooser = jnp.any(
        jnp.arange(expert_count * capacity, dtype=jnp.int32)[:, None, None] == slot_ids[None],
        axis=2,
    ).astype(jnp.bfloat16)
    buffer = jnp.dot(chooser, normed, preferred_element_type=jnp.float32).astype(jnp.bfloat16)
    buffer = buffer.reshape(expert_count, capacity, D)
    arrived = lax.all_to_all(buffer, "sp", split_axis=0, concat_axis=0, tiled=True)
    model_width = arrived.shape[2]
    both_halves = collect(arrived, "tp", 0)
    flat_rows = both_halves.reshape(-1, model_width)
    gate_out = jnp.dot(flat_rows, gate_weight[0], preferred_element_type=jnp.float32)
    upward = jnp.dot(flat_rows, up_weight[0], preferred_element_type=jnp.float32)
    hidden = (jax.nn.silu(gate_out) * upward).astype(jnp.bfloat16)
    partial_value = jnp.dot(hidden, down_weight[0], preferred_element_type=jnp.float32).reshape(
        both_halves.shape
    )
    summed = sum_at_owner(partial_value.astype(jnp.bfloat16), "tp", 0).astype(jnp.bfloat16)
    returned = lax.all_to_all(summed, "sp", split_axis=0, concat_axis=0, tiled=True)
    picked = returned.reshape(-1, D)[slot_ids.reshape(-1)].astype(jnp.float32)
    expert_mix = jnp.sum(
        (picked * route_weight.reshape(-1)[:, None]).reshape(row_count, top_count, D), axis=1
    )
    return (middle.astype(jnp.float32) + expert_mix).astype(jnp.bfloat16)


def solution(mesh):
    in_specs = (
        P(("sp", "tp"), None),
        P("sp", "tp"),
        P("sp", None),
        P("sp", None),
        P("sp"),
        P(None, "tp"),
        P(None, "tp"),
        P(),
        P(),
        P(),
        P(("sp", "tp"), None),
        P(("sp", "tp"), None),
        P("sp", None, "tp"),
        P("sp", None, "tp"),
        P("sp", "tp", None),
    )
    out_specs = P(("sp", "tp"), None)
    return jax.shard_map(local, mesh=mesh, in_specs=in_specs, out_specs=out_specs, check_vma=False)
```

profile of v0, /device:TPU:0, one launch (start us, length us, event | category | flops | bytes accessed | tf_op | source)
XLA Modules:
  0.0 649.7 jit_solution(9027320513454528965)
XLA Ops:
  10.0 1.6 slice.54
  13.5 186.6 %all-gather = s32[64,1,256]{2,1,0:T(1,128)} all-gather(s32[1,1,256]{2,1,0:T(1,128)} %bitcast.92), channel_id=1, replica_groups=mesh['sp'=64,'tp'=2] {'sp'}, dimensions={0}, use_global_device_ids=true | all-gather | bytes 66560 | tf_op jit(solution)/shard_map/all_gather | solution.py:129
  202.9 216.7 %while.17 = (s32[]{:T(128)}, f32[256,6]{0,1:T(8,128)S(1)}, f32[256,6]{0,1:T(8,128)S(1)}, f32[256,6,64]{0,2,1:T(8,128)S(1)}, s32[256]{0:T(256)}, /*index=5*/s32[1...) while((s32[]{:T(128)}, f32[256,6]{0,1:T(8,128)S(1)}, ...), condition=%wide.region_5.6_spmd, body=%wide.region_0.5_spmd.sunk | while | flops 461835776 | bytes 21579896 | solution.py:163
  207.4 1.3 slice.70
  209.5 7.0 %conditional.2 = ((f32[256,6]{0,1:T(8,128)S(1)}, f32[256,6]{0,1:T(8,128)S(1)}, f32[256,6,64]{0,2,1:T(8,128)S(1)})) conditional(s32[]{:T(128)} %convert_element_type.177, (f32[256,6]{0,1:T(8,128)S(1)}, f32[256,6]{0,1:T(8,128)S(1)}, f32[256,6,64]{0,2,1:T(8,128)S(1)}) %tuple.50, (s32[]{:T(128)}, s32[512]{0:T(512)}, s32[256]{0:T(256)}, s32[512]{0:T(512)}, ...), branch_computations={%region_1.0_spmd, %region_2.4_spmd} | conditional | flops 461835776 | bytes 21565132 | solution.py:161
  209.5 1.3 convolution_convert_fusion.1
  210.9 1.5 fusion.16
  221.0 1.3 slice.70
  227.5 1.3 slice.70
  234.1 1.3 slice.70
  421.4 4.0 all_to_all.39
  428.0 137.1 %all_to_all.40 = bf16[64,8,2048]{2,1,0:T(8,128)(2,1)S(1)} all-to-all(bf16[64,8,2048]{2,1,0:T(8,128)(2,1)S(1)} %fusion.23), channel_id=1, replica_groups=mesh['sp'=64,'tp'=2] {'sp'}, dimensions={0} | all-to-all | bytes 4194304 | tf_op jit(solution)/shard_map/all_to_all | solution.py:188
  565.6 7.2 %all_to_all.41 = bf16[2,64,8,2048]{3,2,1,0:T(8,128)(2,1)S(1)} all-to-all(bf16[2,64,8,2048]{3,2,1,0:T(8,128)(2,1)S(1)} %broadcast_in_dim.63), channel_id=1, replica_groups=mesh['sp'=64,'tp'=2] {'tp'}, dimensions={0} | all-to-all | bytes 8388608 | tf_op jit(solution)/shard_map/all_to_all | solution.py:24
  572.8 2.3 fusion.25
  575.2 2.6 fusion.31
  577.8 2.4 convolution_convert_fusion.2
  580.8 8.2 %all_to_all.42 = bf16[2,64,8,2048]{3,1,2,0:T(8,128)(2,1)} all-to-all(bf16[2,64,8,2048]{3,1,2,0:T(8,128)(2,1)S(1)} %copy.65), channel_id=1, replica_groups=mesh['sp'=64,'tp'=2] {'tp'}, dimensions={0} | all-to-all | bytes 8388608 | tf_op jit(solution)/shard_map/all_to_all | solution.py:38
  589.0 3.5 reduce_sum.67
  592.5 2.5 copy.67
  595.0 6.1 all-to-all-start.4
  601.3 29.9 %all-to-all-done.4 = bf16[64,8,2048]{2,1,0:T(8,128)(2,1)S(1)} async-done(((bf16[64,8,2048]{2,1,0:T(8,128)(2,1)}), bf16[64,8,2048]{2,1,0:T(8,128)(2,1)S(1)}, u32[]{:S(2)}, u32[]{:S(2)}) %all-to-all-start.4) | async-done | bytes 2097184 | tf_op jit(solution)/shard_map/all_to_all | solution.py:199
  631.2 2.3 gather_fusion
  633.5 3.5 reshape.226
  637.1 4.9 multiply_reduce_fusion
  (347 shorter events, 159.0 us)
Async XLA Ops:
  6.5 418.9 %copy-start = (bf16[768,2048]{1,0:T(8,128)(2,1)S(1)}, bf16[768,2048]{1,0:T(8,128)(2,1)}, u32[]{:S(2)}) copy-start(bf16[768,2048]{1,0:T(8,128)(2,1)} %param.26) | copy-start | bytes 9437188
  6.5 196.3 %all-gather.6.cloned.1.call-start = ((), (), s32[]{:S(2)}) async-start(), calls=%async_computation.6 | async-start | bytes 1064960 | tf_op jit(solution)/shard_map/all_gather | solution.py:128
  8.2 194.6 %all-gather.4.cloned.1.call-start = ((), (), s32[]{:S(2)}) async-start(), calls=%async_computation.5 | async-start | bytes 8519680 | tf_op jit(solution)/shard_map/all_gather | solution.py:127
  12.6 190.2 %copy-start.14 = (s32[256]{0:T(256)}, s32[256]{0:T(256)S(1)}, u32[]{:S(2)}) copy-start(s32[256]{0:T(256)S(1)} %fusion.49) | copy-start | bytes 3076
  209.5 2.9 copy-start.11
  209.5 2.9 copy-start.10
  209.5 2.9 copy-start.12
  209.5 2.9 copy-start.13
  209.5 3.1 copy-start.4
  213.5 0.9 copy-start.5
  419.7 6.5 copy-start.16
  421.4 4.8 copy-start.6
  425.5 1.7 copy-start.7
  425.5 1.7 copy-start.17
  426.4 0.8 copy-start.2
  565.6 7.2 %copy-start.19 = (bf16[1,2048,512]{2,1,0:T(8,128)(2,1)S(1)}, bf16[1,2048,512]{2,1,0:T(8,128)(2,1)}, u32[]{:S(2)}) copy-start(bf16[1,2048,512]{2,1,0:T(8,128)(2,1)} %param.32) | copy-start | bytes 6291460
  572.8 2.3 copy-start.20
  575.2 2.7 copy-start.21
  595.0 6.1 copy-start.8
  595.0 6.2 copy-start.18
  595.0 6.4 copy-start.15
  595.0 36.2 %all-to-all-start.4 = ((bf16[64,8,2048]{2,1,0:T(8,128)(2,1)}), bf16[64,8,2048]{2,1,0:T(8,128)(2,1)S(1)}, u32[]{:S(2)}, u32[]{:S(2)}) async-start(bf16[64,8,2048]{2,1,0:T(8,128)(2,1)} %copy.67), calls=%async_computation.4 | async-start | bytes 4194304 | tf_op jit(solution)/shard_map/all_to_all | solution.py:199
  633.5 9.3 %copy-start.1 = (bf16[768,2048]{1,0:T(8,128)(2,1)S(1)}, bf16[768,2048]{1,0:T(8,128)(2,1)}, u32[]{:S(2)}) copy-start(bf16[768,2048]{1,0:T(8,128)(2,1)} %param.26) | copy-start | bytes 9437188
  637.1 4.9 copy-start.3
  (32 other events, 19.2 us)
Sparse Core Ops, SparseCore 0:
  10.0 66.1 all-gather.5
  79.0 76.5 all-gather.3
where the time goes:
time: 655 us; the launch traced here: 650 us
  blocking collectives  343 us (52%)
  local copies, waits for them, and re-layouts  160 us (24%)
  loops' own time  64.4 us (10%)
  waiting for transfers between devices  30.6 us (5%)
  other arithmetic  17 us (3%)
  matrix products  14.5 us (2%)
  between operations  13.7 us (2%)
    all_gather x1, blocking collectives, local(): lax.all_gather(doc_ids, 'sp', axis=0, tiled=True)  187 us
    all_to_all x1, blocking collectives, local(): lax.all_to_all(buffer, 'sp', split_axis=0, concat_axis=0, tiled=True)  137 us
    slice x96, local copies, waits for them, and re-layouts, one_block(): active = (first_row <= query_pos[-1]) & (sliced[-1][-1] >= doc_ids[0])  102 us
    another operation x1, loops' own time, local(): running = lax.fori_loop(0, row_count // block_rows, one_block, initial)  63.9 us
    all_to_all x1, waiting for transfers between devices, local(): lax.all_to_all(summed, 'sp', split_axis=0, concat_axis=0, tiled=True)  29.9 us
    dynamic_slice x32, local copies, waits for them, and re-layouts, one_block(): lax.dynamic_slice_in_dim(member, first_row, block_rows, 0)  24.2 us
    iota x32, local copies, waits for them, and re-layouts, one_block(): key_pos = first_row + jnp.arange(block_rows, dtype=jnp.int32)  19.1 us
  transfers between devices with their start and end apart: 3, of which 1 were waited for; matrix products, arithmetic and copies ran while one was open for 1% of the time, Pallas kernels for 0%

commit v1 on v0

--- a/solution.py
+++ b/solution.py
@@ -11,6 +11,18 @@
 GROUPS = 4
 rope_base = 10000.0
 epsilon = 1e-06
+
+
+def doubled_up(x, axis, dim):
+    ways, here = (lax.axis_size(axis), lax.axis_index(axis))
+    grown, reach = (x, 1)
+    while reach < ways:
+        theirs = lax.ppermute(grown, axis, [(d, d ^ reach) for d in range(ways)])
+        mine_first = jnp.concatenate([grown, theirs], axis=dim)
+        theirs_first = jnp.concatenate([theirs, grown], axis=dim)
+        grown = jnp.where(here & reach == 0, mine_first, theirs_first)
+        reach = 2 * reach
+    return grown
 
 
 def in_order(pieces, dim):
@@ -126,7 +138,7 @@
     pieces = (
         lax.all_gather(latent, "sp", axis=0, tiled=True),
         lax.all_gather(key_rot, "sp", axis=0, tiled=True),
-        lax.all_gather(doc_ids, "sp", axis=0, tiled=True),
+        doubled_up(doc_ids, "sp", 0),
     )
     row_count = pieces[0].shape[0]
     block_rows = math.gcd(row_count, 512)

time: 655 us -> 598 us (0.913)
  blocking collectives: 343 us -> 163 us
  waiting for transfers between devices: 30.6 us -> 153 us
  starting transfers between devices: 6.11 us -> 21.8 us
  local copies, waits for them, and re-layouts: 160 us -> 152 us
  loops' own time: 64.4 us -> 56.9 us
    all_gather x1 -> x0, blocking collectives: 187 us -> none  [local(): lax.all_gather(doc_ids, 'sp', axis=0, tiled=True)]
    all_gather x1, waiting for transfers between devices: 0.01 us -> 79.3 us  [local(): lax.all_gather(latent, 'sp', axis=0, tiled=True)]
    all_gather x1, waiting for transfers between devices: 0.01 us -> 38.2 us  [local(): lax.all_gather(key_rot, 'sp', axis=0, tiled=True)]
    ppermute x0 -> x6, starting transfers between devices: none -> 15.7 us  [doubled_up(): theirs = lax.ppermute(grown, axis, [(d, d ^ reach) for d in range(ways)])]
    slice x96, local copies, waits for them, and re-layouts: 102 us -> 94.5 us  [one_block(): active = (first_row <= query_pos[-1]) & (sliced[-1][-1] >= doc_ids[0])]
    another operation x1, loops' own time: 63.9 us -> 56.4 us  [local(): running = lax.fori_loop(0, row_count // block_rows, one_block, initial)]
  transfers between devices with their start and end apart: 3 -> 9, of which waited for: 1 -> 7; matrix products, arithmetic and copies ran while one was open for 1% -> 1% of each run, Pallas kernels for 0% -> 0%
where the time goes in v1:
time: 598 us; the launch traced here: 593 us
  blocking collectives  163 us (27%)
  waiting for transfers between devices  153 us (26%)
  local copies, waits for them, and re-layouts  152 us (25%)
  loops' own time  56.9 us (10%)
  starting transfers between devices  21.8 us (4%)
  other arithmetic  18.3 us (3%)
  matrix products  14.5 us (2%)
  between operations  13.7 us (2%)
    all_to_all x1, blocking collectives, local(): lax.all_to_all(buffer, 'sp', split_axis=0, concat_axis=0, tiled=True)  143 us
    slice x96, local copies, waits for them, and re-layouts, one_block(): active = (first_row <= query_pos[-1]) & (sliced[-1][-1] >= doc_ids[0])  94.5 us
    all_gather x1, waiting for transfers between devices, local(): lax.all_gather(latent, 'sp', axis=0, tiled=True)  79.3 us
    another operation x1, loops' own time, local(): running = lax.fori_loop(0, row_count // block_rows, one_block, initial)  56.4 us
    all_gather x1, waiting for transfers between devices, local(): lax.all_gather(key_rot, 'sp', axis=0, tiled=True)  38.2 us
    all_to_all x1, waiting for transfers between devices, local(): lax.all_to_all(summed, 'sp', split_axis=0, concat_axis=0, tiled=True)  29.9 us
    dynamic_slice x32, local copies, waits for them, and re-layouts, one_block(): lax.dynamic_slice_in_dim(member, first_row, block_rows, 0)  24.2 us
    iota x32, local copies, waits for them, and re-layouts, one_block(): key_pos = first_row + jnp.arange(block_rows, dtype=jnp.int32)  16.7 us
  transfers between devices with their start and end apart: 9, of which 7 were waited for; matrix products, arithmetic and copies ran while one was open for 1% of the time, Pallas kernels for 0%

profile of v1, /device:TPU:0, one launch (start us, length us, event | category | flops | bytes accessed | tf_op | source)
XLA Modules:
  0.0 592.8 jit_solution(16967365003415645047)
XLA Ops:
  9.0 1.7 collective-permute-start
  13.6 3.1 collective-permute-start.1
  18.7 1.7 collective-permute-start.2
  22.3 3.3 collective-permute-start.3
  27.5 2.0 collective-permute-start.4
  31.2 4.0 collective-permute-start.5
  38.0 38.2 %all-gather.5.cloned.1.call-done = bf16[16384,32]{0,1:T(8,128)(2,1)} async-done(((bf16[256,32]{0,1:T(8,128)(2,1)}), bf16[16384,32]{0,1:T(8,128)(2,1)}) %all-gather.5.cloned.1.call-update) | async-done | bytes 1048592 | tf_op jit(solution)/shard_map/all_gather | solution.py:140
  76.2 79.3 %all-gather.3.cloned.1.call-done = bf16[16384,256]{1,0:T(8,128)(2,1)} async-done(((bf16[256,256]{1,0:T(8,128)(2,1)}), bf16[16384,256]{1,0:T(8,128)(2,1)}) %all-gather.3.cloned.1.call-update) | async-done | bytes 8388624 | tf_op jit(solution)/shard_map/all_gather | solution.py:139
  155.6 201.2 %while.17 = (s32[]{:T(128)}, f32[256,6]{0,1:T(8,128)S(1)}, f32[256,6]{0,1:T(8,128)S(1)}, f32[256,6,64]{0,2,1:T(8,128)S(1)}, s32[256]{0:T(256)}, /*index=5*/s32[1...) while((s32[]{:T(128)}, f32[256,6]{0,1:T(8,128)S(1)}, ...), condition=%wide.region_5.6_spmd, body=%wide.region_0.5_spmd.sunk | while | flops 461835776 | bytes 21579896 | solution.py:175
  161.6 7.0 %conditional.2 = ((f32[256,6]{0,1:T(8,128)S(1)}, f32[256,6]{0,1:T(8,128)S(1)}, f32[256,6,64]{0,2,1:T(8,128)S(1)})) conditional(s32[]{:T(128)} %convert_element_type.177, (f32[256,6]{0,1:T(8,128)S(1)}, f32[256,6]{0,1:T(8,128)S(1)}, f32[256,6,64]{0,2,1:T(8,128)S(1)}) %tuple.50, (s32[]{:T(128)}, s32[512]{0:T(512)}, s32[256]{0:T(256)}, s32[512]{0:T(512)}, ...), branch_computations={%region_1.1_spmd, %region_2.4_spmd} | conditional | flops 461835776 | bytes 21565132 | solution.py:173
  358.6 4.0 all_to_all.39
  365.1 143.1 %all_to_all.40 = bf16[64,8,2048]{2,1,0:T(8,128)(2,1)S(1)} all-to-all(bf16[64,8,2048]{2,1,0:T(8,128)(2,1)S(1)} %fusion.23), channel_id=1, replica_groups=mesh['sp'=64,'tp'=2] {'sp'}, dimensions={0} | all-to-all | bytes 4194304 | tf_op jit(solution)/shard_map/all_to_all | solution.py:200
  508.8 7.2 %all_to_all.41 = bf16[2,64,8,2048]{3,2,1,0:T(8,128)(2,1)S(1)} all-to-all(bf16[2,64,8,2048]{3,2,1,0:T(8,128)(2,1)S(1)} %broadcast_in_dim.63), channel_id=1, replica_groups=mesh['sp'=64,'tp'=2] {'tp'}, dimensions={0} | all-to-all | bytes 8388608 | tf_op jit(solution)/shard_map/all_to_all | solution.py:36
  516.0 2.3 fusion.25
  518.4 2.6 fusion.31
  521.1 2.4 convolution_convert_fusion.2
  524.0 8.1 %all_to_all.42 = bf16[2,64,8,2048]{3,1,2,0:T(8,128)(2,1)} all-to-all(bf16[2,64,8,2048]{3,1,2,0:T(8,128)(2,1)S(1)} %copy.65), channel_id=1, replica_groups=mesh['sp'=64,'tp'=2] {'tp'}, dimensions={0} | all-to-all | bytes 8388608 | tf_op jit(solution)/shard_map/all_to_all | solution.py:50
  532.2 3.5 reduce_sum.67
  535.6 2.5 copy.67
  538.1 6.1 %all-to-all-start.4 = ((bf16[64,8,2048]{2,1,0:T(8,128)(2,1)}), bf16[64,8,2048]{2,1,0:T(8,128)(2,1)S(1)}, u32[]{:S(2)}, u32[]{:S(2)}) async-start(bf16[64,8,2048]{2,1,0:T(8,128)(2,1)} %copy.67), calls=%async_computation.4 | async-start | bytes 4194304 | tf_op jit(solution)/shard_map/all_to_all | solution.py:211
  544.5 29.9 %all-to-all-done.4 = bf16[64,8,2048]{2,1,0:T(8,128)(2,1)S(1)} async-done(((bf16[64,8,2048]{2,1,0:T(8,128)(2,1)}), bf16[64,8,2048]{2,1,0:T(8,128)(2,1)S(1)}, u32[]{:S(2)}, u32[]{:S(2)}) %all-to-all-start.4) | async-done | bytes 2097184 | tf_op jit(solution)/shard_map/all_to_all | solution.py:211
  574.4 2.3 gather_fusion
  576.7 3.5 reshape.226
  580.2 4.9 multiply_reduce_fusion
  (364 shorter events, 166.9 us)
Async XLA Ops:
  6.5 356.1 %copy-start = (bf16[768,2048]{1,0:T(8,128)(2,1)S(1)}, bf16[768,2048]{1,0:T(8,128)(2,1)}, u32[]{:S(2)}) copy-start(bf16[768,2048]{1,0:T(8,128)(2,1)} %param.26) | copy-start | bytes 9437188
  6.5 69.6 %all-gather.5.cloned.1.call-start = ((), (), s32[]{:S(2)}) async-start(), calls=%async_computation.6 | async-start | bytes 1064960 | tf_op jit(solution)/shard_map/all_gather | solution.py:140
  8.2 147.3 %all-gather.3.cloned.1.call-start = ((), (), s32[]{:S(2)}) async-start(), calls=%async_computation.5 | async-start | bytes 8519680 | tf_op jit(solution)/shard_map/all_gather | solution.py:139
  9.0 3.9 collective-permute-start
  12.7 63.5 %copy-start.14 = (s32[256]{0:T(256)}, s32[256]{0:T(256)S(1)}, u32[]{:S(2)}) copy-start(s32[256]{0:T(256)S(1)} %fusion.49) | copy-start | bytes 3076
  13.6 5.1 collective-permute-start.1
  18.7 3.6 collective-permute-start.2
  22.3 5.2 collective-permute-start.3
  27.5 3.7 collective-permute-start.4
  31.2 6.2 %collective-permute-start.5 = (s32[8192]{0:T(1024)S(1)}, s32[8192]{0:T(1024)S(1)}, u32[]{:S(2)}, u32[]{:S(2)}) collective-permute-start(s32[8192]{0:T(1024)S(1)} %add_select_fusion.1), channel_id=1, source_target_pairs={{0,64},{2,66},{4,68},{6,70},{8,72},{10,74},{12,76},{14,78},{16,80}... | collective-permute-start | bytes 98312 | tf_op jit(solution)/shard_map/ppermute | solution.py:20
  161.6 2.9 copy-start.11
  161.6 2.9 copy-start.10
  161.6 2.9 copy-start.12
  161.7 2.9 copy-start.13
  161.7 3.1 copy-start.4
  356.8 6.5 %copy-start.16 = (f32[2048]{0:T(1024)S(1)}, f32[2048]{0:T(1024)}, u32[]{:S(2)}) copy-start(f32[2048]{0:T(1024)} %param.27) | copy-start | bytes 24580
  358.5 4.8 copy-start.6
  508.8 7.2 %copy-start.19 = (bf16[1,2048,512]{2,1,0:T(8,128)(2,1)S(1)}, bf16[1,2048,512]{2,1,0:T(8,128)(2,1)}, u32[]{:S(2)}) copy-start(bf16[1,2048,512]{2,1,0:T(8,128)(2,1)} %param.32) | copy-start | bytes 6291460
  538.1 6.1 %copy-start.8 = (s32[128,2]{1,0:T(8,128)S(1)}, s32[128,2]{1,0:T(8,128)}, u32[]{:S(2)}) copy-start(s32[128,2]{1,0:T(8,128)} %get-tuple-element.385) | copy-start | bytes 3076
  538.1 6.2 %copy-start.18 = (f32[128,2]{0,1:T(2,128)S(1)}, f32[128,2]{0,1:T(2,128)}, u32[]{:S(2)}) copy-start(f32[128,2]{0,1:T(2,128)} %param.30) | copy-start | bytes 3076
  538.1 6.4 %copy-start.15 = (s32[256]{0:T(256)S(1)}, s32[256]{0:T(256)}, u32[]{:S(2)}) copy-start(s32[256]{0:T(256)} %copy-done.14) | copy-start | bytes 3076
  538.1 36.2 %all-to-all-start.4 = ((bf16[64,8,2048]{2,1,0:T(8,128)(2,1)}), bf16[64,8,2048]{2,1,0:T(8,128)(2,1)S(1)}, u32[]{:S(2)}, u32[]{:S(2)}) async-start(bf16[64,8,2048]{2,1,0:T(8,128)(2,1)} %copy.67), calls=%async_computation.4 | async-start | bytes 4194304 | tf_op jit(solution)/shard_map/all_to_all | solution.py:211
  576.7 9.3 %copy-start.1 = (bf16[768,2048]{1,0:T(8,128)(2,1)S(1)}, bf16[768,2048]{1,0:T(8,128)(2,1)}, u32[]{:S(2)}) copy-start(bf16[768,2048]{1,0:T(8,128)(2,1)} %param.26) | copy-start | bytes 9437188
  580.2 4.9 copy-start.3
  (38 other events, 29.1 us)
Sparse Core Ops, SparseCore 0:
  10.0 66.1 all-gather.4
  79.0 76.4 all-gather.2
